TPU v7x, 256 devices: a whole 4x4x8 slice. The times are simulated.
256 devices in a mesh: kv: 16 (over y, x), tp: 16 (over z, core).
Axes of the slice: x: 4, y: 4, z: 8, core: 2. Of those that a mesh axis runs over, the one named last changes fastest.
Arguments:
- tokens: bfloat16 [256, 4096], P('kv', 'tp'), may hold values from -6 to 6
- attn_gain: float32 [4096], replicated, may hold values from 0.1 to 1.9
- w_query: bfloat16 [4096, 2048], P(None, 'tp'), may hold values from -0.09375 to 0.09375
- w_key: bfloat16 [4096, 2048], P(None, 'tp'), may hold values from -0.09375 to 0.09375
- w_value: bfloat16 [4096, 2048], P(None, 'tp'), may hold values from -0.09375 to 0.09375
- w_outgate: bfloat16 [4096, 2048], P(None, 'tp'), may hold values from -0.09375 to 0.09375
- w_rates: bfloat16 [2, 4096, 16], P(None, None, 'tp'), may hold values from -0.09375 to 0.09375
- head_rate: float32 [16], P('tp'), may hold values from 0.02 to 2
- head_gain: float32 [2048], P('tp'), may hold values from 0.1 to 1.9
- w_out: bfloat16 [2048, 4096], P('tp'), may hold values from -0.125 to 0.125
- state: float32 [256, 16, 128, 128], P('kv', 'tp'), may hold values from -2.4 to 2.4
- mlp_gain: float32 [4096], replicated, may hold values from 0.1 to 1.9
- w_gate: bfloat16 [4096, 11264], P(None, ('kv', 'tp')), may hold values from -0.09375 to 0.09375
- w_up: bfloat16 [4096, 11264], P(None, ('kv', 'tp')), may hold values from -0.09375 to 0.09375
- w_down: bfloat16 [4096, 11264], P(None, ('kv', 'tp')), may hold values from -0.25 to 0.25
Outputs:
- result: bfloat16 [256, 4096], P('kv', 'tp')
- new_state: float32 [256, 16, 128, 128], P('kv', 'tp')
All inputs are finite; a program needn't handle non-finite values.
Results may differ from a plain program's by a relative error of at most 0.014.
Values may be sent and summed in bfloat16 or wider, within the bound.
No kernel may reach another device: no remote copies, remote signals or barrier semaphores. Data moves between devices by JAX's collectives and lax.ppermute only.
A program may use at most 64 MiB of HBM per device.

v0:
```python
import jax
import jax.numpy as jnp
from jax import lax
from jax.sharding import PartitionSpec as P

EPS = 1e-06


def copy_for_each(value, axis):
    size = lax.axis_size(axis)
    return lax.all_to_all(
        jnp.broadcast_to(value[None], (size, *value.shape)), axis, 0, 0, tiled=True
    )


def in_order(tiles, dim):
    lengths = list(tiles.shape[1:])
    lengths[dim] *= tiles.shape[0]
    return jnp.moveaxis(tiles, 0, dim).reshape(lengths)


def gather_directly(value, axis, dim):
    tiles = copy_for_each(value, axis)
    return in_order(tiles, dim)


def cut_along(value, dim, size):
    lengths = value.shape
    tiles = value.reshape(*lengths[:dim], size, lengths[dim] // size, *lengths[dim + 1 :])
    return jnp.moveaxis(tiles, dim, 0)


def sent_and_summed(value, axis, dim):
    size = lax.axis_size(axis)
    tiles = lax.all_to_all(cut_along(value, dim, size), axis, 0, 0, tiled=True)
    return jnp.sum(tiles.astype(jnp.float32), axis=0)


def sent_and_summed_2(value, axis, dim):
    tiles = cut_along(value, dim, lax.axis_size(axis))
    arrived = lax.all_to_all(tiles, axis, split_axis=0, concat_axis=0, tiled=True)
    return arrived.sum(axis=0)


def row_norm(values, gain):
    floats = values.astype(jnp.float32)
    scaled = floats * lax.rsqrt(jnp.mean(floats * floats, axis=-1, keepdims=True) + EPS)
    return (scaled * gain).astype(jnp.bfloat16)


def hidden_units(normed_mlp, gate_part, up_part):
    gate_pre = jnp.dot(normed_mlp, gate_part, preferred_element_type=jnp.float32)
    up_pre = jnp.dot(normed_mlp, up_part, preferred_element_type=jnp.float32)
    return (jax.nn.silu(gate_pre) * up_pre).astype(jnp.bfloat16)


def down_product(hidden, down_part):
    return lax.dot_general(
        hidden, down_part, (((1,), (1,)), ((), ())), preferred_element_type=jnp.float32
    )


def body(
    tokens,
    attn_gain,
    w_query,
    w_key,
    w_value,
    w_outgate,
    w_rates,
    head_rate,
    head_gain,
    w_out,
    state,
    mlp_gain,
    w_gate,
    w_up,
    w_down,
):
    count = tokens.shape[0]
    local_heads = head_rate.shape[0]
    size = w_query.shape[1] // local_heads
    whole_rows = gather_directly(tokens, "tp", 1)
    normed = row_norm(whole_rows, attn_gain)
    query = jnp.dot(normed, w_query, preferred_element_type=jnp.float32).reshape(
        count, local_heads, size
    )
    key = jnp.dot(normed, w_key, preferred_element_type=jnp.float32).reshape(
        count, local_heads, size
    )
    value = jnp.dot(normed, w_value, preferred_element_type=jnp.float32).reshape(
        count, local_heads, size
    )
    gate_in = jnp.dot(normed, w_outgate, preferred_element_type=jnp.float32).reshape(
        count, local_heads, size
    )
    rates = jnp.einsum("bd,sdh->sbh", normed, w_rates, preferred_element_type=jnp.float32)
    unit_query = (
        query * lax.rsqrt(jnp.sum(query * query, axis=-1, keepdims=True) + EPS) * size ** (-0.5)
    )
    unit_key = key * lax.rsqrt(jnp.sum(key * key, axis=-1, keepdims=True) + EPS)
    strength = jax.nn.sigmoid(rates[0])
    fade = jnp.exp(-head_rate * jax.nn.softplus(rates[1]))
    carried = state * fade[:, :, None, None]
    fresh = strength[:, :, None] * (value - jnp.einsum("bhi,bhiv->bhv", unit_key, carried))
    new_state = carried + unit_key[:, :, :, None] * fresh[:, :, None, :]
    readout = jnp.einsum("bhi,bhiv->bhv", unit_query, new_state)
    normed_out = readout * lax.rsqrt(jnp.mean(readout * readout, axis=-1, keepdims=True) + EPS)
    mixed = (normed_out * head_gain.reshape(local_heads, size) * jax.nn.silu(gate_in)).astype(
        jnp.bfloat16
    )
    partial_value = jnp.dot(
        mixed.reshape(count, local_heads * size), w_out, preferred_element_type=jnp.float32
    )
    projected = sent_and_summed(partial_value.astype(jnp.bfloat16), "tp", 1)
    residual = (tokens.astype(jnp.float32) + projected).astype(jnp.bfloat16)
    full_residual = gather_directly(residual, "tp", 1)
    normed_mlp = row_norm(full_residual, mlp_gain)
    shared_rows = gather_directly(normed_mlp, "kv", 0)
    hidden = hidden_units(shared_rows, w_gate, w_up)
    owned = lax.all_to_all(hidden, "kv", split_axis=0, concat_axis=1, tiled=True)
    folded = down_product(owned, lax.all_gather(w_down, "kv", axis=1, tiled=True))
    down = sent_and_summed_2(folded, "tp", 1)
    result = (residual.astype(jnp.float32) + down).astype(jnp.bfloat16)
    return (result, new_state)


def solution(mesh):
    return jax.shard_map(
        body,
        mesh=mesh,
        in_specs=(
            P("kv", "tp"),
            P(),
            P(None, "tp"),
            P(None, "tp"),
            P(None, "tp"),
            P(None, "tp"),
            P(None, None, "tp"),
            P("tp"),
            P("tp"),
            P("tp", None),
            P("kv", "tp", None, None),
            P(),
            P(None, ("kv", "tp")),
            P(None, ("kv", "tp")),
            P(None, ("kv", "tp")),
        ),
        out_specs=(P("kv", "tp"), P("kv", "tp", None, None)),
        check_vma=False,
    )
```

profile of v0, /device:TPU:1, one launch (start us, length us, event | category | flops | bytes accessed | tf_op | source)
XLA Modules:
  0.0 156.5 jit_solution(1678312154421125208)
XLA Ops:
  7.2 0.0 copy-start
  7.2 0.0 copy-start.8
  7.2 0.0 copy-start.2
  7.2 0.0 all-gather.3.cloned.1.call-start
  7.2 0.7 all-gather.3.cloned.1.call-update
  7.9 1.4 broadcast_in_dim.6
  9.3 10.0 %all-to-all-start = ((bf16[16,16,256]{2,1,0:T(8,128)(2,1)}), bf16[16,16,256]{2,1,0:T(8,128)(2,1)S(1)}, u32[]{:S(2)}, u32[]{:S(2)}) async-start(bf16[16,16,256]{2,1,0:T(8,128)(2,1)} %broadcast_in_dim.6), calls=%async_computation | async-start | bytes 262144 | tf_op jit(solution)/shard_map/all_to_all | solution.py:11
  19.9 0.7 mul.205
  20.6 7.5 %all-to-all-done = bf16[16,16,256]{2,1,0:T(8,128)(2,1)S(1)} async-done(((bf16[16,16,256]{2,1,0:T(8,128)(2,1)}), bf16[16,16,256]{2,1,0:T(8,128)(2,1)S(1)}, u32[]{:S(2)}, u32[]{:S(2)}) %all-to-all-start) | async-done | bytes 131104 | tf_op jit(solution)/shard_map/all_to_all | solution.py:11
  28.2 0.0 copy-start.3
  28.2 0.1 fusion.15
  28.3 0.0 copy-start.12
  28.3 0.1 fusion.18
  28.4 0.0 copy-start.1
  28.5 0.0 copy-start.4
  28.5 0.0 copy-done.8
  28.5 0.1 multiply_convert_fusion.1
  28.6 0.0 copy-done.2
  28.6 0.4 multiply_reduce_fusion.1
  29.0 0.4 copy-done.3
  29.4 0.0 copy-start.5
  29.4 0.0 copy-start.11
  29.4 0.4 multiply_reduce_fusion.2
  29.8 0.0 copy-done.12
  29.8 0.2 convolution_bitcast_fusion
  30.0 0.1 broadcast_multiply_fusion
  30.1 0.1 multiply_multiply_fusion
  30.1 0.0 copy-done.1
  30.1 0.3 fusion.10
  30.4 0.0 copy-done.4
  30.4 0.3 fusion.7
  30.7 0.0 copy-start.9
  30.7 0.5 fusion.33
  31.2 0.1 multiply_reduce_fusion
  31.3 0.0 copy-done
  31.3 0.0 copy-done.5
  31.3 0.0 copy-done.11
  31.4 0.0 copy-start.10
  31.4 0.5 convolution_convert_fusion
  31.9 11.6 %all_to_all.44 = bf16[16,16,256]{2,1,0:T(8,128)(2,1)S(1)} all-to-all(bf16[16,16,256]{2,1,0:T(8,128)(2,1)S(1)} %bitcast.108), channel_id=1, replica_groups=mesh['kv'=16,'tp'=16] {'tp'}, dimensions={0} | all-to-all | bytes 262144 | tf_op jit(solution)/shard_map/all_to_all | solution.py:35
  43.5 0.0 copy-done.9
  43.5 11.6 %all_to_all.45 = bf16[16,16,256]{2,1,0:T(8,128)(2,1)S(1)} all-to-all(bf16[16,16,256]{2,1,0:T(8,128)(2,1)S(1)} %broadcast_in_dim.7), channel_id=1, replica_groups=mesh['kv'=16,'tp'=16] {'tp'}, dimensions={0} | all-to-all | bytes 262144 | tf_op jit(solution)/shard_map/all_to_all | solution.py:11
  55.1 0.1 fusion.14
  55.3 0.0 copy-done.10
  55.3 0.1 multiply_convert_fusion
  55.4 0.2 broadcast_in_dim.8
  55.6 0.0 copy-start.6
  55.6 49.6 %all_to_all.46 = bf16[16,16,4096]{2,1,0:T(8,128)(2,1)S(1)} all-to-all(bf16[16,16,4096]{2,1,0:T(8,128)(2,1)S(1)} %broadcast_in_dim.8), channel_id=1, replica_groups=mesh['kv'=16,'tp'=16] {'kv'}, dimensions={0} | all-to-all | bytes 4194304 | tf_op jit(solution)/shard_map/all_to_all | solution.py:11
  105.2 0.0 copy-done.6
  105.2 0.7 fusion.36
  106.0 0.2 copy-done.7
  106.2 0.7 fusion.6
  107.0 0.1 copy.25
  107.1 0.1 reshape.265
  107.3 9.0 %all_to_all.47 = bf16[16,2,352]{2,1,0:T(2,128)(2,1)S(1)} all-to-all(bf16[16,2,352]{2,1,0:T(2,128)(2,1)S(1)} %reshape.265), channel_id=1, replica_groups=mesh['kv'=16,'tp'=16] {'kv'}, dimensions={0} | all-to-all | bytes 45056 | tf_op jit(solution)/shard_map/all_to_all | solution.py:121
  116.3 0.1 reshape.266
  116.4 0.1 reshape.263
  116.5 0.0 all-gather.3.cloned.1.call-done
  116.5 8.0 %reshape.258 = bf16[704,4096]{1,0:T(8,128)(2,1)} reshape(bf16[16,44,4096]{2,1,0:T(8,128)(2,1)} %all-gather.3.cloned.1.call-done) | data formatting | bytes 11534336
  124.6 4.2 %fusion.3 = f32[16,16,256]{2,1,0:T(8,128)} fusion(bf16[16,704,1]{1,0,2:T(8,128)(2,1)S(1)} %reshape.263, bf16[88,16,8,256]{3,2,1,0:T(8,128)(2,1)} %bitcast.102), kind=kOutput, calls=%fused_computation.4 | convolution fusion | flops 92274688 | bytes 6051840 | tf_op jit(solution)/shard_map/dot_general | solution.py:58
  128.8 8.7 %all-to-all-start.5 = ((f32[16,16,256]{2,1,0:T(8,128)}), f32[16,16,256]{2,1,0:T(8,128)S(1)}, u32[]{:S(2)}, u32[]{:S(2)}) async-start(f32[16,16,256]{2,1,0:T(8,128)} %fusion.3), calls=%async_computation.5 | async-start | bytes 524288 | tf_op jit(solution)/shard_map/all_to_all | solution.py:41
  137.5 1.3 multiply_add_fusion
  138.8 10.3 %all-to-all-done.5 = f32[16,16,256]{2,1,0:T(8,128)S(1)} async-done(((f32[16,16,256]{2,1,0:T(8,128)}), f32[16,16,256]{2,1,0:T(8,128)S(1)}, u32[]{:S(2)}, u32[]{:S(2)}) %all-to-all-start.5) | async-done | bytes 262176 | tf_op jit(solution)/shard_map/all_to_all | solution.py:41
  149.1 0.6 add_convert_fusion
  (19 shorter events, 0.3 us)
Async XLA Ops:
  7.2 24.2 %copy-start = (bf16[128,4096]{1,0:T(8,128)(2,1)S(1)}, bf16[128,4096]{1,0:T(8,128)(2,1)}, u32[]{:S(2)}) copy-start(bf16[128,4096]{1,0:T(8,128)(2,1)} %param.24) | copy-start | bytes 3145732
  7.2 21.3 %copy-start.8 = (f32[4096]{0:T(1024)S(1)}, f32[4096]{0:T(1024)}, u32[]{:S(2)}) copy-start(f32[4096]{0:T(1024)} %param.16) | copy-start | bytes 49156
  7.2 21.4 %copy-start.2 = (bf16[4096,128]{1,0:T(8,128)(2,1)S(1)}, bf16[4096,128]{1,0:T(8,128)(2,1)}, u32[]{:S(2)}) copy-start(bf16[4096,128]{1,0:T(8,128)(2,1)} %param.18) | copy-start | bytes 3145732
  7.2 109.3 %all-gather.3.cloned.1.call-start = ((), (), s32[]{:S(2)}) async-start(), calls=%async_computation.6 | async-start | bytes 6684672 | tf_op jit(solution)/shard_map/all_gather | solution.py:122
  9.3 18.9 %all-to-all-start = ((bf16[16,16,256]{2,1,0:T(8,128)(2,1)}), bf16[16,16,256]{2,1,0:T(8,128)(2,1)S(1)}, u32[]{:S(2)}, u32[]{:S(2)}) async-start(bf16[16,16,256]{2,1,0:T(8,128)(2,1)} %broadcast_in_dim.6), calls=%async_computation | async-start | bytes 262144 | tf_op jit(solution)/shard_map/all_to_all | solution.py:11
  28.2 1.2 copy-start.3
  28.3 1.4 copy-start.12
  28.4 1.7 %copy-start.1 = (f32[16,1,128,128]{3,2,1,0:T(8,128)S(1)}, f32[16,1,128,128]{3,2,1,0:T(8,128)}, u32[]{:S(2)}) copy-start(f32[16,1,128,128]{3,2,1,0:T(8,128)} %param.25) | copy-start | bytes 3145732
  28.5 1.9 %copy-start.4 = (bf16[4096,128]{1,0:T(8,128)(2,1)S(1)}, bf16[4096,128]{1,0:T(8,128)(2,1)}, u32[]{:S(2)}) copy-start(bf16[4096,128]{1,0:T(8,128)(2,1)} %param.19) | copy-start | bytes 3145732
  29.4 2.0 %copy-start.5 = (bf16[4096,128]{1,0:T(8,128)(2,1)S(1)}, bf16[4096,128]{1,0:T(8,128)(2,1)}, u32[]{:S(2)}) copy-start(bf16[4096,128]{1,0:T(8,128)(2,1)} %param.20) | copy-start | bytes 3145732
  29.4 2.0 %copy-start.11 = (f32[128]{0:T(128)S(1)}, f32[128]{0:T(128)}, u32[]{:S(2)}) copy-start(f32[128]{0:T(128)} %param.23) | copy-start | bytes 1540
  30.7 12.8 %copy-start.9 = (bf16[16,256]{1,0:T(8,128)(2,1)S(1)}, bf16[16,256]{1,0:T(8,128)(2,1)}, u32[]{:S(2)}) copy-start(bf16[16,256]{1,0:T(8,128)(2,1)} %param.15) | copy-start | bytes 24580
  31.4 23.9 %copy-start.10 = (f32[4096]{0:T(1024)S(1)}, f32[4096]{0:T(1024)}, u32[]{:S(2)}) copy-start(f32[4096]{0:T(1024)} %param.26) | copy-start | bytes 49156
  55.6 49.6 %copy-start.6 = (bf16[4096,44]{0,1:T(8,128)(2,1)S(1)}, bf16[4096,44]{0,1:T(8,128)(2,1)}, u32[]{:S(2)}) copy-start(bf16[4096,44]{0,1:T(8,128)(2,1)} %param.27) | copy-start | bytes 1081348
  105.2 1.0 copy-start.7
  128.8 20.3 %all-to-all-start.5 = ((f32[16,16,256]{2,1,0:T(8,128)}), f32[16,16,256]{2,1,0:T(8,128)S(1)}, u32[]{:S(2)}, u32[]{:S(2)}) async-start(f32[16,16,256]{2,1,0:T(8,128)} %fusion.3), calls=%async_computation.5 | async-start | bytes 524288 | tf_op jit(solution)/shard_map/all_to_all | solution.py:41
Sparse Core Ops, SparseCore 0:
  10.4 91.6 all-gather.2
where the time goes:
time: 157 us
  blocking collectives  81.7 us (52%)
  starting transfers between devices  18.7 us (12%)
  waiting for transfers between devices  18.5 us (12%)
  between operations  15 us (10%)
  local copies, waits for them, and re-layouts  11.6 us (7%)
  matrix products  8.08 us (5%)
  other arithmetic  2.96 us (2%)
    all_to_all x2, blocking collectives, copy_for_each(): lax.all_to_all(jnp.broadcast_to(value[None], (size, *value.shape)), axis,...  61.2 us
    all_to_all x1, blocking collectives, sent_and_summed(): tiles = lax.all_to_all(cut_along(value, dim, size), axis, 0, 0, tiled=True)  11.6 us
    all_to_all x1, waiting for transfers between devices, sent_and_summed_2(): lax.all_to_all(tiles, axis, split_axis=0, concat_axis=0, tiled=True)  10.3 us
    all_to_all x1, starting transfers between devices, copy_for_each(): lax.all_to_all(jnp.broadcast_to(value[None], (size, *value.shape)), axis,...  9.97 us
    all_to_all x1, blocking collectives, body(): lax.all_to_all(hidden, 'kv', split_axis=0, concat_axis=1, tiled=True)  8.99 us
    unnamed x29, local copies, waits for them, and re-layouts  8.94 us
    all_to_all x1, starting transfers between devices, sent_and_summed_2(): lax.all_to_all(tiles, axis, split_axis=0, concat_axis=0, tiled=True)  8.69 us
    all_to_all x1, waiting for transfers between devices, copy_for_each(): lax.all_to_all(jnp.broadcast_to(value[None], (size, *value.shape)), axis,...  7.51 us
  transfers between devices with their start and end apart: 3, of which 2 were waited for; matrix products, arithmetic and copies ran while one was open for 6% of the time, Pallas kernels for 0%

commit v1 on v0

--- a/solution.py
+++ b/solution.py
@@ -2,6 +2,7 @@
 import jax.numpy as jnp
 from jax import lax
 from jax.sharding import PartitionSpec as P
+from jax.lax import axis_index, ppermute, psum
 
 EPS = 1e-06
 
@@ -118,7 +119,23 @@
     normed_mlp = row_norm(full_residual, mlp_gain)
     shared_rows = gather_directly(normed_mlp, "kv", 0)
     hidden = hidden_units(shared_rows, w_gate, w_up)
-    owned = lax.all_to_all(hidden, "kv", split_axis=0, concat_axis=1, tiled=True)
+
+    def direct_seats_all_on_mesh(load, comm_axis, pos_dim, which_dim):
+        u_next, last = (psum(1, comm_axis), axis_index(comm_axis))
+        b_next = list(load.shape)
+        ready = load.shape[pos_dim] // u_next
+        b_next[pos_dim] = ready
+        z = b_next[which_dim]
+        b_next[which_dim] = z * u_next
+        small = jnp.zeros(b_next, load.dtype)
+        for t in range(u_next):
+            big = lax.dynamic_slice_in_dim(load, (last ^ t) * ready, ready, axis=pos_dim)
+            if t:
+                big = ppermute(big, comm_axis, [(dev_j, dev_j ^ t) for dev_j in range(u_next)])
+            small = lax.dynamic_update_slice_in_dim(small, big, (last ^ t) * z, axis=which_dim)
+        return small
+
+    owned = direct_seats_all_on_mesh(hidden, comm_axis="kv", pos_dim=0, which_dim=1)
     folded = down_product(owned, lax.all_gather(w_down, "kv", axis=1, tiled=True))
     down = sent_and_summed_2(folded, "tp", 1)
     result = (residual.astype(jnp.float32) + down).astype(jnp.bfloat16)

time: 157 us -> 180 us (1.15)
  blocking collectives: 81.7 us -> 23.1 us
  waiting for transfers between devices: 18.5 us -> 61.7 us
  starting transfers between devices: 18.7 us -> 51.2 us
  local copies, waits for them, and re-layouts: 11.6 us -> 17.3 us
    all_to_all x2 -> x1, blocking collectives: 61.2 us -> 11.6 us  [copy_for_each(): lax.all_to_all(jnp.broadcast_to(value[None], (size, *value.shape)), axis,...]
    all_to_all x1 -> x2, waiting for transfers between devices: 7.51 us -> 50.7 us  [copy_for_each(): lax.all_to_all(jnp.broadcast_to(value[None], (size, *value.shape)), axis,...]
    ppermute x0 -> x15, starting transfers between devices: none -> 24.2 us  [direct_seats_all_on_mesh(): ppermute(big, comm_axis, [(dev_j, dev_j ^ t) for dev_j in range(u_next)])]
    all_to_all x1 -> x0, blocking collectives: 8.99 us -> none  [body(): lax.all_to_all(hidden, 'kv', split_axis=0, concat_axis=1, tiled=True)]
    all_to_all x1 -> x2, starting transfers between devices: 9.97 us -> 16.9 us  [copy_for_each(): lax.all_to_all(jnp.broadcast_to(value[None], (size, *value.shape)), axis,...]
    dynamic_update_slice x0 -> x16, local copies, waits for them, and re-layouts: none -> 3.67 us  [direct_seats_all_on_mesh(): lax.dynamic_update_slice_in_dim(small, big, (last ^ t) * z, axis=which_dim)]
    unnamed x29 -> x37, local copies, waits for them, and re-layouts: 8.94 us -> 8.94 us
  transfers between devices with their start and end apart: 3 -> 19, of which waited for: 2 -> 3; matrix products, arithmetic and copies ran while one was open for 6% -> 8% of each run, Pallas kernels for 0% -> 0%
where the time goes in v1:
time: 180 us; the launch traced here: 179 us
  waiting for transfers between devices  61.7 us (34%)
  starting transfers between devices  51.2 us (28%)
  blocking collectives  23.1 us (13%)
  local copies, waits for them, and re-layouts  17.3 us (10%)
  between operations  15.4 us (9%)
  matrix products  7.48 us (4%)
  other arithmetic  2.96 us (2%)
    all_to_all x2, waiting for transfers between devices, copy_for_each(): lax.all_to_all(jnp.broadcast_to(value[None], (size, *value.shape)), axis,...  50.7 us
    ppermute x15, starting transfers between devices, direct_seats_all_on_mesh(): ppermute(big, comm_axis, [(dev_j, dev_j ^ t) for dev_j in range(u_next)])  24.2 us
    all_to_all x2, starting transfers between devices, copy_for_each(): lax.all_to_all(jnp.broadcast_to(value[None], (size, *value.shape)), axis,...  16.9 us
    all_to_all x1, blocking collectives, sent_and_summed(): tiles = lax.all_to_all(cut_along(value, dim, size), axis, 0, 0, tiled=True)  11.6 us
    all_to_all x1, blocking collectives, copy_for_each(): lax.all_to_all(jnp.broadcast_to(value[None], (size, *value.shape)), axis,...  11.6 us
    all_to_all x1, waiting for transfers between devices, sent_and_summed_2(): lax.all_to_all(tiles, axis, split_axis=0, concat_axis=0, tiled=True)  10.2 us
    all_to_all x1, starting transfers between devices, sent_and_summed_2(): lax.all_to_all(tiles, axis, split_axis=0, concat_axis=0, tiled=True)  10.2 us
    unnamed x37, local copies, waits for them, and re-layouts  8.94 us
  transfers between devices with their start and end apart: 19, of which 3 were waited for; matrix products, arithmetic and copies ran while one was open for 8% of the time, Pallas kernels for 0%

profile of v1, /device:TPU:1, one launch (start us, length us, event | category | flops | bytes accessed | tf_op | source)
XLA Modules:
  0.0 179.2 jit_solution(17767848905073000115)
XLA Ops:
  7.3 0.7 all-gather.3.cloned.1.call-update
  7.9 1.4 broadcast_in_dim.8
  9.3 10.0 %all-to-all-start = ((bf16[16,16,256]{2,1,0:T(8,128)(2,1)}), bf16[16,16,256]{2,1,0:T(8,128)(2,1)S(1)}, u32[]{:S(2)}, u32[]{:S(2)}) async-start(bf16[16,16,256]{2,1,0:T(8,128)(2,1)} %broadcast_in_dim.8), calls=%async_computation | async-start | bytes 262144 | tf_op jit(solution)/shard_map/all_to_all | solution.py:12
  19.9 0.7 mul.301
  20.7 7.5 %all-to-all-done = bf16[16,16,256]{2,1,0:T(8,128)(2,1)S(1)} async-done(((bf16[16,16,256]{2,1,0:T(8,128)(2,1)}), bf16[16,16,256]{2,1,0:T(8,128)(2,1)S(1)}, u32[]{:S(2)}, u32[]{:S(2)}) %all-to-all-start) | async-done | bytes 131104 | tf_op jit(solution)/shard_map/all_to_all | solution.py:12
  28.2 0.1 fusion.9
  28.3 0.1 fusion.12
  28.5 0.1 multiply_convert_fusion.1
  28.7 0.4 multiply_reduce_fusion.1
  29.1 0.4 multiply_reduce_fusion.2
  29.4 0.1 convolution_bitcast_fusion
  29.8 0.3 fusion.4
  30.1 0.3 fusion.1
  30.4 0.5 fusion.27
  30.9 0.1 multiply_reduce_fusion
  31.1 0.5 convolution_convert_fusion
  31.6 11.6 %all_to_all.25 = bf16[16,16,256]{2,1,0:T(8,128)(2,1)S(1)} all-to-all(bf16[16,16,256]{2,1,0:T(8,128)(2,1)S(1)} %bitcast.105), channel_id=1, replica_groups=mesh['kv'=16,'tp'=16] {'tp'}, dimensions={0} | all-to-all | bytes 262144 | tf_op jit(solution)/shard_map/all_to_all | solution.py:36
  43.2 0.6 copy-done.9
  43.8 11.6 %all_to_all.26 = bf16[16,16,256]{2,1,0:T(8,128)(2,1)S(1)} all-to-all(bf16[16,16,256]{2,1,0:T(8,128)(2,1)S(1)} %broadcast_in_dim.10), channel_id=1, replica_groups=mesh['kv'=16,'tp'=16] {'tp'}, dimensions={0} | all-to-all | bytes 262144 | tf_op jit(solution)/shard_map/all_to_all | solution.py:12
  55.4 0.1 fusion.8
  55.6 0.1 multiply_convert_fusion
  55.7 1.6 broadcast_in_dim.11
  57.3 6.9 %all-to-all-start.3 = ((bf16[16,16,4096]{2,1,0:T(8,128)(2,1)}), bf16[16,16,4096]{2,1,0:T(8,128)(2,1)S(1)}, u32[]{:S(2)}, u32[]{:S(2)}) async-start(bf16[16,16,4096]{2,1,0:T(8,128)(2,1)} %broadcast_in_dim.11), calls=%async_computation.3 | async-start | bytes 4194304 | tf_op jit(solution)/shard_map/all_to_all | solution.py:12
  64.3 43.2 %all-to-all-done.3 = bf16[16,16,4096]{2,1,0:T(8,128)(2,1)S(1)} async-done(((bf16[16,16,4096]{2,1,0:T(8,128)(2,1)}), bf16[16,16,4096]{2,1,0:T(8,128)(2,1)S(1)}, u32[]{:S(2)}, u32[]{:S(2)}) %all-to-all-start.3) | async-done | bytes 2097184 | tf_op jit(solution)/shard_map/all_to_all | solution.py:12
  107.5 0.7 fusion.30
  108.3 0.2 copy-done.8
  108.5 0.7 fusion
  109.3 0.2 constant_dynamic-slice_fusion
  109.5 1.4 collective-permute-start.8
  110.9 2.2 %collective-permute-start.7 = (bf16[16,44]{0,1:T(8,128)(2,1)S(1)}, bf16[16,44]{0,1:T(8,128)(2,1)S(1)}, u32[]{:S(2)}, u32[]{:S(2)}) collective-permute-start(bf16[16,44]{0,1:T(8,128)(2,1)S(1)} %get-tuple-element.9), channel_id=1, source_target_pairs={{0,128},{16,144},{32,160},{48,176},{64,192},{80,208},{96,224},{112... | collective-permute-start | bytes 4232 | tf_op jit(solution)/shard_map/ppermute | solution.py:134
  113.2 3.2 %collective-permute-start.6 = (bf16[16,44]{0,1:T(8,128)(2,1)S(1)}, bf16[16,44]{0,1:T(8,128)(2,1)S(1)}, u32[]{:S(2)}, u32[]{:S(2)}) collective-permute-start(bf16[16,44]{0,1:T(8,128)(2,1)S(1)} %get-tuple-element.10), channel_id=1, source_target_pairs={{0,112},{16,96},{32,80},{48,64},{64,48},{80,32},{96,16},{112,0},{1... | collective-permute-start | bytes 4232 | tf_op jit(solution)/shard_map/ppermute | solution.py:134
  116.4 1.1 collective-permute-start.5
  117.4 0.3 collective-permute-start.4
  117.7 0.8 collective-permute-start.3
  118.5 2.6 %collective-permute-start.2 = (bf16[16,44]{0,1:T(8,128)(2,1)S(1)}, bf16[16,44]{0,1:T(8,128)(2,1)S(1)}, u32[]{:S(2)}, u32[]{:S(2)}) collective-permute-start(bf16[16,44]{0,1:T(8,128)(2,1)S(1)} %get-tuple-element.14), channel_id=1, source_target_pairs={{0,48},{16,32},{32,16},{48,0},{64,112},{80,96},{96,80},{112,64},{1... | collective-permute-start | bytes 4232 | tf_op jit(solution)/shard_map/ppermute | solution.py:134
  121.1 1.5 collective-permute-start.1
  122.6 2.4 %collective-permute-start.12 = (bf16[16,44]{0,1:T(8,128)(2,1)S(1)}, bf16[16,44]{0,1:T(8,128)(2,1)S(1)}, u32[]{:S(2)}, u32[]{:S(2)}) collective-permute-start(bf16[16,44]{0,1:T(8,128)(2,1)S(1)} %get-tuple-element.4), channel_id=1, source_target_pairs={{0,208},{16,192},{32,240},{48,224},{64,144},{80,128},{96,176},{112... | collective-permute-start | bytes 4232 | tf_op jit(solution)/shard_map/ppermute | solution.py:134
  125.0 2.9 %collective-permute-start.10 = (bf16[16,44]{0,1:T(8,128)(2,1)S(1)}, bf16[16,44]{0,1:T(8,128)(2,1)S(1)}, u32[]{:S(2)}, u32[]{:S(2)}) collective-permute-start(bf16[16,44]{0,1:T(8,128)(2,1)S(1)} %get-tuple-element.6), channel_id=1, source_target_pairs={{0,176},{16,160},{32,144},{48,128},{64,240},{80,224},{96,208},{112... | collective-permute-start | bytes 4232 | tf_op jit(solution)/shard_map/ppermute | solution.py:134
  127.8 1.8 %collective-permute-start.11 = (bf16[16,44]{0,1:T(8,128)(2,1)S(1)}, bf16[16,44]{0,1:T(8,128)(2,1)S(1)}, u32[]{:S(2)}, u32[]{:S(2)}) collective-permute-start(bf16[16,44]{0,1:T(8,128)(2,1)S(1)} %get-tuple-element.5), channel_id=1, source_target_pairs={{0,192},{16,208},{32,224},{48,240},{64,128},{80,144},{96,160},{112... | collective-permute-start | bytes 4232 | tf_op jit(solution)/shard_map/ppermute | solution.py:134
  129.6 0.5 collective-permute-start.13
  130.2 3.5 %collective-permute-start.14 = (bf16[16,44]{0,1:T(8,128)(2,1)S(1)}, bf16[16,44]{0,1:T(8,128)(2,1)S(1)}, u32[]{:S(2)}, u32[]{:S(2)}) collective-permute-start(bf16[16,44]{0,1:T(8,128)(2,1)S(1)} %get-tuple-element.2), channel_id=1, source_target_pairs={{0,240},{16,224},{32,208},{48,192},{64,176},{80,160},{96,144},{112... | collective-permute-start | bytes 4232 | tf_op jit(solution)/shard_map/ppermute | solution.py:134
  133.7 0.2 dynamic_update_slice.48
  133.9 0.2 dynamic_update_slice.49
  134.2 0.2 dynamic_update_slice.50
  134.4 0.2 dynamic_update_slice.51
  134.6 0.2 dynamic_update_slice.52
  134.9 0.2 dynamic_update_slice.53
  135.1 0.2 dynamic_update_slice.54
  135.3 0.2 dynamic_update_slice.55
  135.6 0.2 dynamic_update_slice.56
  135.8 0.2 dynamic_update_slice.57
  136.1 0.2 dynamic_update_slice.58
  136.3 0.2 dynamic_update_slice.59
  136.6 0.2 dynamic_update_slice.60
  136.8 0.2 dynamic_update_slice.61
  137.0 0.3 dynamic_update_slice.62
  137.3 0.2 dynamic_update_slice.63
  137.6 8.0 %reshape.257 = bf16[704,4096]{1,0:T(8,128)(2,1)} reshape(bf16[16,44,4096]{2,1,0:T(8,128)(2,1)} %all-gather.3.cloned.1.call-done) | data formatting | bytes 11534336
  145.6 3.6 %fusion.31 = f32[16,4096]{1,0:T(8,128)S(1)} fusion(bf16[16,704]{0,1:T(8,128)(2,1)S(1)} %dynamic_update_slice.63, bf16[704,4096]{1,0:T(8,128)(2,1)} %reshape.257), kind=kOutput, calls=%fused_computation.76 | convolution fusion | flops 92274688 | bytes 6051840 | tf_op jit(solution)/shard_map/dot_general | solution.py:59
  149.2 0.7 copy.33
  149.9 10.2 %all-to-all-start.4 = ((f32[16,16,256]{2,1,0:T(8,128)}), f32[16,16,256]{2,1,0:T(8,128)S(1)}, u32[]{:S(2)}, u32[]{:S(2)}) async-start(f32[16,16,256]{2,1,0:T(8,128)} %bitcast.96), calls=%async_computation.4 | async-start | bytes 524288 | tf_op jit(solution)/shard_map/all_to_all | solution.py:42
  160.1 1.3 multiply_add_fusion
  161.5 10.2 %all-to-all-done.4 = f32[16,16,256]{2,1,0:T(8,128)S(1)} async-done(((f32[16,16,256]{2,1,0:T(8,128)}), f32[16,16,256]{2,1,0:T(8,128)S(1)}, u32[]{:S(2)}, u32[]{:S(2)}) %all-to-all-start.4) | async-done | bytes 262176 | tf_op jit(solution)/shard_map/all_to_all | solution.py:42
  171.7 0.6 add_convert_fusion
  (73 shorter events, 0.7 us)
Async XLA Ops:
  7.2 23.8 %copy-start = (bf16[128,4096]{1,0:T(8,128)(2,1)S(1)}, bf16[128,4096]{1,0:T(8,128)(2,1)}, u32[]{:S(2)}) copy-start(bf16[128,4096]{1,0:T(8,128)(2,1)} %param.24) | copy-start | bytes 3145732
  7.2 21.4 %copy-start.11 = (f32[4096]{0:T(1024)S(1)}, f32[4096]{0:T(1024)}, u32[]{:S(2)}) copy-start(f32[4096]{0:T(1024)} %param.16) | copy-start | bytes 49156
  7.2 21.5 %copy-start.3 = (bf16[4096,128]{1,0:T(8,128)(2,1)S(1)}, bf16[4096,128]{1,0:T(8,128)(2,1)}, u32[]{:S(2)}) copy-start(bf16[4096,128]{1,0:T(8,128)(2,1)} %param.18) | copy-start | bytes 3145732
  7.2 21.8 %copy-start.4 = (bf16[4096,128]{1,0:T(8,128)(2,1)S(1)}, bf16[4096,128]{1,0:T(8,128)(2,1)}, u32[]{:S(2)}) copy-start(bf16[4096,128]{1,0:T(8,128)(2,1)} %param.17) | copy-start | bytes 3145732
  7.2 130.3 %all-gather.3.cloned.1.call-start = ((), (), s32[]{:S(2)}) async-start(), calls=%async_computation.5 | async-start | bytes 6684672 | tf_op jit(solution)/shard_map/all_gather | solution.py:139
  9.3 18.9 %all-to-all-start = ((bf16[16,16,256]{2,1,0:T(8,128)(2,1)}), bf16[16,16,256]{2,1,0:T(8,128)(2,1)S(1)}, u32[]{:S(2)}, u32[]{:S(2)}) async-start(bf16[16,16,256]{2,1,0:T(8,128)(2,1)} %broadcast_in_dim.8), calls=%async_computation | async-start | bytes 262144 | tf_op jit(solution)/shard_map/all_to_all | solution.py:12
  28.3 1.1 copy-start.17
  28.4 1.4 copy-start.1
  28.5 1.6 copy-start.5
  29.0 2.0 %copy-start.6 = (bf16[4096,128]{1,0:T(8,128)(2,1)S(1)}, bf16[4096,128]{1,0:T(8,128)(2,1)}, u32[]{:S(2)}) copy-start(bf16[4096,128]{1,0:T(8,128)(2,1)} %param.20) | copy-start | bytes 3145732
  29.0 2.0 %copy-start.16 = (f32[128]{0:T(128)S(1)}, f32[128]{0:T(128)}, u32[]{:S(2)}) copy-start(f32[128]{0:T(128)} %param.23) | copy-start | bytes 1540
  29.6 1.4 copy-start.14
  30.4 12.8 %copy-start.12 = (bf16[16,256]{1,0:T(8,128)(2,1)S(1)}, bf16[16,256]{1,0:T(8,128)(2,1)}, u32[]{:S(2)}) copy-start(bf16[16,256]{1,0:T(8,128)(2,1)} %param.15) | copy-start | bytes 24580
  31.0 24.5 %copy-start.13 = (f32[4096]{0:T(1024)S(1)}, f32[4096]{0:T(1024)}, u32[]{:S(2)}) copy-start(f32[4096]{0:T(1024)} %param.26) | copy-start | bytes 49156
  43.2 0.6 copy-start.9
  57.3 50.2 %copy-start.7 = (bf16[4096,44]{0,1:T(8,128)(2,1)S(1)}, bf16[4096,44]{0,1:T(8,128)(2,1)}, u32[]{:S(2)}) copy-start(bf16[4096,44]{0,1:T(8,128)(2,1)} %param.27) | copy-start | bytes 1081348
  57.3 50.2 %all-to-all-start.3 = ((bf16[16,16,4096]{2,1,0:T(8,128)(2,1)}), bf16[16,16,4096]{2,1,0:T(8,128)(2,1)S(1)}, u32[]{:S(2)}, u32[]{:S(2)}) async-start(bf16[16,16,4096]{2,1,0:T(8,128)(2,1)} %broadcast_in_dim.11), calls=%async_computation.3 | async-start | bytes 4194304 | tf_op jit(solution)/shard_map/all_to_all | solution.py:12
  107.5 1.0 copy-start.8
  109.4 8.0 %collective-permute-start.9 = (bf16[16,44]{0,1:T(8,128)(2,1)S(1)}, bf16[16,44]{0,1:T(8,128)(2,1)S(1)}, u32[]{:S(2)}, u32[]{:S(2)}) collective-permute-start(bf16[16,44]{0,1:T(8,128)(2,1)S(1)} %get-tuple-element.7), channel_id=1, source_target_pairs={{0,160},{16,176},{32,128},{48,144},{64,224},{80,240},{96,192},{112... | collective-permute-start | bytes 4232 | tf_op jit(solution)/shard_map/ppermute | solution.py:134
  109.5 8.1 %collective-permute-start.8 = (bf16[16,44]{0,1:T(8,128)(2,1)S(1)}, bf16[16,44]{0,1:T(8,128)(2,1)S(1)}, u32[]{:S(2)}, u32[]{:S(2)}) collective-permute-start(bf16[16,44]{0,1:T(8,128)(2,1)S(1)} %get-tuple-element.8), channel_id=1, source_target_pairs={{0,144},{16,128},{32,176},{48,160},{64,208},{80,192},{96,240},{112... | collective-permute-start | bytes 4232 | tf_op jit(solution)/shard_map/ppermute | solution.py:134
  110.9 7.6 %collective-permute-start.7 = (bf16[16,44]{0,1:T(8,128)(2,1)S(1)}, bf16[16,44]{0,1:T(8,128)(2,1)S(1)}, u32[]{:S(2)}, u32[]{:S(2)}) collective-permute-start(bf16[16,44]{0,1:T(8,128)(2,1)S(1)} %get-tuple-element.9), channel_id=1, source_target_pairs={{0,128},{16,144},{32,160},{48,176},{64,192},{80,208},{96,224},{112... | collective-permute-start | bytes 4232 | tf_op jit(solution)/shard_map/ppermute | solution.py:134
  113.2 7.9 %collective-permute-start.6 = (bf16[16,44]{0,1:T(8,128)(2,1)S(1)}, bf16[16,44]{0,1:T(8,128)(2,1)S(1)}, u32[]{:S(2)}, u32[]{:S(2)}) collective-permute-start(bf16[16,44]{0,1:T(8,128)(2,1)S(1)} %get-tuple-element.10), channel_id=1, source_target_pairs={{0,112},{16,96},{32,80},{48,64},{64,48},{80,32},{96,16},{112,0},{1... | collective-permute-start | bytes 4232 | tf_op jit(solution)/shard_map/ppermute | solution.py:134
  116.4 6.2 %collective-permute-start.5 = (bf16[16,44]{0,1:T(8,128)(2,1)S(1)}, bf16[16,44]{0,1:T(8,128)(2,1)S(1)}, u32[]{:S(2)}, u32[]{:S(2)}) collective-permute-start(bf16[16,44]{0,1:T(8,128)(2,1)S(1)} %get-tuple-element.11), channel_id=1, source_target_pairs={{0,96},{16,112},{32,64},{48,80},{64,32},{80,48},{96,0},{112,16},{1... | collective-permute-start | bytes 4232 | tf_op jit(solution)/shard_map/ppermute | solution.py:134
  117.4 5.1 %collective-permute-start.4 = (bf16[16,44]{0,1:T(8,128)(2,1)S(1)}, bf16[16,44]{0,1:T(8,128)(2,1)S(1)}, u32[]{:S(2)}, u32[]{:S(2)}) collective-permute-start(bf16[16,44]{0,1:T(8,128)(2,1)S(1)} %get-tuple-element.12), channel_id=1, source_target_pairs={{0,80},{16,64},{32,112},{48,96},{64,16},{80,0},{96,48},{112,32},{1... | collective-permute-start | bytes 4232 | tf_op jit(solution)/shard_map/ppermute | solution.py:134
  117.7 7.3 %collective-permute-start.3 = (bf16[16,44]{0,1:T(8,128)(2,1)S(1)}, bf16[16,44]{0,1:T(8,128)(2,1)S(1)}, u32[]{:S(2)}, u32[]{:S(2)}) collective-permute-start(bf16[16,44]{0,1:T(8,128)(2,1)S(1)} %get-tuple-element.13), channel_id=1, source_target_pairs={{0,64},{16,80},{32,96},{48,112},{64,0},{80,16},{96,32},{112,48},{1... | collective-permute-start | bytes 4232 | tf_op jit(solution)/shard_map/ppermute | solution.py:134
  118.5 9.3 %collective-permute-start.2 = (bf16[16,44]{0,1:T(8,128)(2,1)S(1)}, bf16[16,44]{0,1:T(8,128)(2,1)S(1)}, u32[]{:S(2)}, u32[]{:S(2)}) collective-permute-start(bf16[16,44]{0,1:T(8,128)(2,1)S(1)} %get-tuple-element.14), channel_id=1, source_target_pairs={{0,48},{16,32},{32,16},{48,0},{64,112},{80,96},{96,80},{112,64},{1... | collective-permute-start | bytes 4232 | tf_op jit(solution)/shard_map/ppermute | solution.py:134
  121.1 8.6 %collective-permute-start.1 = (bf16[16,44]{0,1:T(8,128)(2,1)S(1)}, bf16[16,44]{0,1:T(8,128)(2,1)S(1)}, u32[]{:S(2)}, u32[]{:S(2)}) collective-permute-start(bf16[16,44]{0,1:T(8,128)(2,1)S(1)} %get-tuple-element.15), channel_id=1, source_target_pairs={{0,32},{16,48},{32,0},{48,16},{64,96},{80,112},{96,64},{112,80},{1... | collective-permute-start | bytes 4232 | tf_op jit(solution)/shard_map/ppermute | solution.py:134
  122.6 7.6 %collective-permute-start = (bf16[16,44]{0,1:T(8,128)(2,1)S(1)}, bf16[16,44]{0,1:T(8,128)(2,1)S(1)}, u32[]{:S(2)}, u32[]{:S(2)}) collective-permute-start(bf16[16,44]{0,1:T(8,128)(2,1)S(1)} %get-tuple-element.16), channel_id=1, source_target_pairs={{0,16},{16,0},{32,48},{48,32},{64,80},{80,64},{96,112},{112,96},{1... | collective-permute-start | bytes 4232 | tf_op jit(solution)/shard_map/ppermute | solution.py:134
  122.6 14.2 %collective-permute-start.12 = (bf16[16,44]{0,1:T(8,128)(2,1)S(1)}, bf16[16,44]{0,1:T(8,128)(2,1)S(1)}, u32[]{:S(2)}, u32[]{:S(2)}) collective-permute-start(bf16[16,44]{0,1:T(8,128)(2,1)S(1)} %get-tuple-element.4), channel_id=1, source_target_pairs={{0,208},{16,192},{32,240},{48,224},{64,144},{80,128},{96,176},{112... | collective-permute-start | bytes 4232 | tf_op jit(solution)/shard_map/ppermute | solution.py:134
  125.0 11.3 %collective-permute-start.10 = (bf16[16,44]{0,1:T(8,128)(2,1)S(1)}, bf16[16,44]{0,1:T(8,128)(2,1)S(1)}, u32[]{:S(2)}, u32[]{:S(2)}) collective-permute-start(bf16[16,44]{0,1:T(8,128)(2,1)S(1)} %get-tuple-element.6), channel_id=1, source_target_pairs={{0,176},{16,160},{32,144},{48,128},{64,240},{80,224},{96,208},{112... | collective-permute-start | bytes 4232 | tf_op jit(solution)/shard_map/ppermute | solution.py:134
  127.8 8.7 %collective-permute-start.11 = (bf16[16,44]{0,1:T(8,128)(2,1)S(1)}, bf16[16,44]{0,1:T(8,128)(2,1)S(1)}, u32[]{:S(2)}, u32[]{:S(2)}) collective-permute-start(bf16[16,44]{0,1:T(8,128)(2,1)S(1)} %get-tuple-element.5), channel_id=1, source_target_pairs={{0,192},{16,208},{32,224},{48,240},{64,128},{80,144},{96,160},{112... | collective-permute-start | bytes 4232 | tf_op jit(solution)/shard_map/ppermute | solution.py:134
  129.6 7.4 %collective-permute-start.13 = (bf16[16,44]{0,1:T(8,128)(2,1)S(1)}, bf16[16,44]{0,1:T(8,128)(2,1)S(1)}, u32[]{:S(2)}, u32[]{:S(2)}) collective-permute-start(bf16[16,44]{0,1:T(8,128)(2,1)S(1)} %get-tuple-element.3), channel_id=1, source_target_pairs={{0,224},{16,240},{32,192},{48,208},{64,160},{80,176},{96,128},{112... | collective-permute-start | bytes 4232 | tf_op jit(solution)/shard_map/ppermute | solution.py:134
  130.2 7.2 %collective-permute-start.14 = (bf16[16,44]{0,1:T(8,128)(2,1)S(1)}, bf16[16,44]{0,1:T(8,128)(2,1)S(1)}, u32[]{:S(2)}, u32[]{:S(2)}) collective-permute-start(bf16[16,44]{0,1:T(8,128)(2,1)S(1)} %get-tuple-element.2), channel_id=1, source_target_pairs={{0,240},{16,224},{32,208},{48,192},{64,176},{80,160},{96,144},{112... | collective-permute-start | bytes 4232 | tf_op jit(solution)/shard_map/ppermute | solution.py:134
  145.6 14.5 %copy-start.2 = (f32[16,1,128,128]{3,2,1,0:T(8,128)S(1)}, f32[16,1,128,128]{3,2,1,0:T(8,128)}, u32[]{:S(2)}) copy-start(f32[16,1,128,128]{3,2,1,0:T(8,128)} %param.25) | copy-start | bytes 3145732
  145.6 14.5 %copy-start.15 = (f32[16]{0:T(128)S(1)}, f32[16]{0:T(128)}, u32[]{:S(2)}) copy-start(f32[16]{0:T(128)} %copy-done.14) | copy-start | bytes 196
  149.2 22.5 %copy-start.10 = (bf16[16,256]{1,0:T(8,128)(2,1)S(1)}, bf16[16,256]{1,0:T(8,128)(2,1)}, u32[]{:S(2)}) copy-start(bf16[16,256]{1,0:T(8,128)(2,1)} %copy-done.9) | copy-start | bytes 24580
  149.9 21.8 %all-to-all-start.4 = ((f32[16,16,256]{2,1,0:T(8,128)}), f32[16,16,256]{2,1,0:T(8,128)S(1)}, u32[]{:S(2)}, u32[]{:S(2)}) async-start(f32[16,16,256]{2,1,0:T(8,128)} %bitcast.96), calls=%async_computation.4 | async-start | bytes 524288 | tf_op jit(solution)/shard_map/all_to_all | solution.py:42
Sparse Core Ops, SparseCore 0:
  10.4 91.0 all-gather.2
